TPU v7x, 32 devices: a whole 2x2x4 slice. The times are simulated.
32 devices in a mesh: grp: 2 (over x), tp: 4 (over z), dp: 4 (over y, core).
Axes of the slice: x: 2, y: 2, z: 4, core: 2. Of those that a mesh axis runs over, the one named last changes fastest.
Arguments:
- tokens: bfloat16 [32, 4096], P(('grp', 'tp'), 'dp'), parts along dimension 0, may hold values from -30 to 30
- norm_gain: float32 [2, 4096], P(None, 'dp'), may hold values from 0.1 to 1.9
- w_query: bfloat16 [2, 4096, 2048], P(None, 'dp', 'tp'), may hold values from -0.09375 to 0.09375
- w_forget: bfloat16 [2, 4096, 2048], P(None, 'dp', 'tp'), may hold values from -0.09375 to 0.09375
- w_value: bfloat16 [2, 4096, 2048], P(None, 'dp', 'tp'), may hold values from -0.09375 to 0.09375
- w_gate: bfloat16 [2, 4096, 2048], P(None, 'dp', 'tp'), may hold values from -0.09375 to 0.09375
- lower_bound: float32 [2, 2048], P(None, 'tp'), may hold values from 0 to 0.9
- head_gain: float32 [2, 128], replicated, may hold values from 0.1 to 1.9
- w_out: bfloat16 [2, 2048, 4096], P(None, 'tp', 'dp'), may hold values from -0.125 to 0.125
- state: float32 [2, 32, 16, 128, 128], P(None, ('grp', 'dp'), 'tp'), parts along dimension 1, may hold values from -4 to 4
Outputs:
- hidden_out: bfloat16 [32, 4096], P(('grp', 'tp'), 'dp'), parts along dimension 0
- new_state: float32 [2, 32, 16, 128, 128], P(None, ('grp', 'dp'), 'tp'), parts along dimension 1
There are 2 independent parts, one for each index of `grp`. A program takes and returns all parts, laid end to end along the dimension named above; an argument that names none is the same for every part. Nothing has to cross between parts.
All inputs are finite; a program needn't handle non-finite values.
Results may differ from a plain program's by a relative error of at most 0.02.
Values may be sent and summed in bfloat16 or wider, within the bound.
No kernel may reach another device: no remote copies, remote signals or barrier semaphores. Data moves between devices by JAX's collectives and lax.ppermute only.
A program may use at most 64 MiB of HBM per device.

v0:
```python
import jax
import jax.numpy as jnp
from jax import lax
from jax.sharding import PartitionSpec as P

D = 4096
HD = 128


def per_device(
    tokens, norm_gain, w_query, w_forget, w_value, w_gate, lower_bound, head_gain, w_out, state
):
    local_seqs = state.shape[1]
    head_count = state.shape[2]
    offset = lax.axis_index("dp") * local_seqs
    hidden = tokens
    updated = []
    for layer in range(2):
        gathered = lax.all_gather(hidden, "tp", axis=0, tiled=True)
        widened = gathered.astype(jnp.float32)
        squares = jnp.sum(widened * widened, axis=1)
        scaled = (widened * norm_gain[layer]).astype(jnp.bfloat16)
        joined = jnp.concatenate(
            [
                jnp.dot(scaled, weight[layer], preferred_element_type=jnp.float32)
                for weight in (w_query, w_forget, w_value, w_gate)
            ],
            axis=1,
        )
        square_total = lax.psum(squares, "dp")
        own_squares = lax.dynamic_slice_in_dim(square_total, offset, local_seqs, 0)
        payload = (joined,)
        summed = (lax.psum(payload[0].astype(jnp.bfloat16), "dp").astype(jnp.float32),)
        shares = tuple(
            (lax.dynamic_slice_in_dim(member, offset, local_seqs, 0) for member in summed)
        )
        own_proj = shares[0]
        width = own_proj.shape[1] // 4
        factor = lax.rsqrt(own_squares / D + 1e-06)[:, None]
        query, forget_pre, value, gate_pre = (
            own_proj[:, index * width : (index + 1) * width] * factor for index in range(4)
        )
        bound = lower_bound[layer]
        forget = bound + (1.0 - bound) * jax.nn.sigmoid(forget_pre)
        keyvec = (1.0 - bound) * jax.nn.sigmoid(-forget_pre)

        def shaped(array):
            return array.reshape(local_seqs, head_count, HD)

        carried = (
            shaped(forget)[..., None] * state[layer]
            + shaped(keyvec)[..., None] * shaped(value)[..., None, :]
        )
        updated.append(carried)
        readout = jnp.einsum("bhkv,bhk->bhv", carried, shaped(query))
        readout = (
            readout
            * lax.rsqrt(jnp.mean(readout * readout, axis=-1, keepdims=True) + 1e-06)
            * head_gain[layer]
        )
        normed = (readout.reshape(local_seqs, head_count * HD) * jax.nn.sigmoid(gate_pre)).astype(
            jnp.bfloat16
        )
        out_weight = w_out[layer]
        mixed = jnp.dot(
            lax.all_gather(normed, "dp", axis=0, tiled=True),
            out_weight,
            preferred_element_type=jnp.float32,
        )
        mixed_sum = lax.psum_scatter(
            mixed.astype(jnp.bfloat16), "tp", scatter_dimension=0, tiled=True
        ).astype(jnp.float32)
        hidden = (hidden.astype(jnp.float32) + mixed_sum).astype(jnp.bfloat16)
    return (hidden, jnp.stack(updated))


def solution(mesh):
    return jax.shard_map(
        per_device,
        mesh=mesh,
        in_specs=(
            P(("grp", "tp"), "dp"),
            P(None, "dp"),
            P(None, "dp", "tp"),
            P(None, "dp", "tp"),
            P(None, "dp", "tp"),
            P(None, "dp", "tp"),
            P(None, "tp"),
            P(),
            P(None, "tp", "dp"),
            P(None, ("grp", "dp"), "tp", None, None),
        ),
        out_specs=(P(("grp", "tp"), "dp"), P(None, ("grp", "dp"), "tp", None, None)),
        check_vma=False,
    )
```

profile of v0, /device:TPU:0, one launch (start us, length us, event | category | flops | bytes accessed | tf_op | source)
XLA Modules:
  0.0 181.9 jit_solution(1064112044140529132)
XLA Ops:
  7.2 0.0 copy-start.1
  7.2 0.0 all-reduce.5.cloned.1.call-start
  7.2 0.9 fusion.47
  8.1 15.1 %all-gather = bf16[4,4,1024]{2,1,0:T(4,128)(2,1)S(1)} all-gather(bf16[1,4,1024]{2,1,0:T(4,128)(2,1)} %bitcast.92), channel_id=1, replica_groups=mesh['grp'=2,'tp'=4,'dp'=4] {'tp'}, dimensions={0}, use_global_device_ids=true | all-gather | bytes 40960 | tf_op jit(solution)/shard_map/all_gather | solution.py:19
  23.2 0.1 multiply_convert_fusion.1
  23.3 0.0 copy-start.6
  23.3 0.0 copy-start.5
  23.3 0.0 copy-start.7
  23.3 1.5 convolution_convert_fusion.6
  24.8 1.5 convolution_convert_fusion.7
  26.3 0.0 copy-done.1
  26.3 0.3 convolution_convert_fusion.8
  26.5 0.0 copy-start.4
  26.5 0.0 copy-start
  26.5 1.6 convolution_convert_fusion.9
  28.2 0.7 pad_maximum_fusion.1
  28.8 0.0 all-reduce.5.cloned.1.call-update
  28.8 0.0 all-reduce.7.cloned.1.call-start
  28.9 0.0 copy-done.6
  28.9 0.0 copy-done.5
  28.9 5.7 %psum.29 = f32[16]{0:T(128)S(1)} all-reduce(f32[16]{0:T(128)S(1)} %get-tuple-element.7), channel_id=1, replica_groups=mesh['grp'=2,'tp'=4,'dp'=4] {'dp'}, use_global_device_ids=true, to_apply=%region_2.0 | all-reduce | flops 16 | bytes 128 | tf_op jit(solution)/shard_map/psum | solution.py:30
  34.6 0.1 add_rsqrt_fusion.3
  34.7 0.0 copy-done.7
  34.7 0.6 dynamic-slice
  35.9 25.6 %all-reduce.5.cloned.1.call-done = bf16[16,2048]{1,0:T(8,128)(2,1)} async-done(((bf16[16,2048]{1,0:T(8,128)(2,1)}), bf16[16,2048]{1,0:T(8,128)(2,1)}) %all-reduce.5.cloned.1.call-update) | async-done | bytes 65552 | tf_op jit(solution)/shard_map/psum | solution.py:33
  61.5 0.8 dynamic-slice_convert_fusion.1
  62.3 0.1 multiply_add_fusion.3
  62.4 1.9 %fusion.10 = f32[4,4,1,128]{3,2,1,0:T(1,128)S(1)} fusion(f32[4,4,128,1]{2,3,1,0:T(1,128)S(1)} %bitcast.100, f32[2,4,4,128,128]{4,3,2,1,0:T(8,128)} %param.19, f32[4,4,128]{2,1,0:T(4,128)S(1)} %mul.268, f32[4,4,128]{2,1,0:T(4,128)S(1)} %mul.265, f32[4,4,128]{2,1,0:T(4,128)S(1)} %mul.261), kind=kOutput, calls=%fused_computation.22 | convolution fusion | flops 1310720 | bytes 1089536 | tf_op jit(solution)/shard_map/bhkv,bhk->bhv/dot_general | solution.py:55
  64.4 0.1 multiply_reduce_fusion.3
  64.5 0.1 multiply_bitcast_fusion.1
  64.5 0.1 fusion.45
  64.6 5.2 %all-gather.1 = bf16[4,4,512]{2,1,0:T(4,128)(2,1)S(1)} all-gather(bf16[1,4,512]{2,1,0:T(4,128)(2,1)S(1)} %fusion.45), channel_id=1, replica_groups=mesh['grp'=2,'tp'=4,'dp'=4] {'dp'}, dimensions={0}, use_global_device_ids=true | all-gather | bytes 20480 | tf_op jit(solution)/shard_map/all_gather | solution.py:66
  69.9 1.5 convolution_convert_fusion.1
  71.3 19.0 %all-reduce = bf16[16,1024]{1,0:T(8,128)(2,1)S(1)} all-reduce(bf16[16,1024]{1,0:T(8,128)(2,1)S(1)} %convolution_convert_fusion.1), channel_id=2, replica_groups=mesh['grp'=2,'tp'=4,'dp'=4] {'tp'}, use_global_device_ids=true, to_apply=%region_4.0.clone | all-reduce | flops 16384 | bytes 65536
  90.3 0.0 copy-done.4
  90.4 13.1 %all-gather.2 = bf16[4,4,1024]{2,1,0:T(4,128)(2,1)S(1)} all-gather(bf16[1,4,1024]{2,1,0:T(4,128)(2,1)S(1)} %fusion.46), channel_id=1, replica_groups=mesh['grp'=2,'tp'=4,'dp'=4] {'tp'}, dimensions={0}, use_global_device_ids=true | all-gather | bytes 40960 | tf_op jit(solution)/shard_map/all_gather | solution.py:19
  103.5 0.0 copy-start.2
  103.5 0.1 multiply_convert_fusion
  103.6 0.0 copy-done
  103.6 0.2 convolution_convert_fusion.2
  103.9 1.7 convolution_convert_fusion.3
  105.6 0.0 copy-done.2
  105.6 0.3 convolution_convert_fusion.4
  105.8 1.5 convolution_convert_fusion.5
  107.3 5.9 %psum.31 = f32[16]{0:T(128)S(1)} all-reduce(f32[16]{0:T(128)S(1)} %get-tuple-element.5), channel_id=1, replica_groups=mesh['grp'=2,'tp'=4,'dp'=4] {'dp'}, use_global_device_ids=true, to_apply=%region_7.0 | all-reduce | flops 16 | bytes 128 | tf_op jit(solution)/shard_map/psum | solution.py:30
  113.1 0.6 pad_maximum_fusion.2
  113.8 0.0 all-reduce.7.cloned.1.call-update
  113.8 0.1 add_rsqrt_fusion.2
  113.9 28.8 %all-reduce.7.cloned.1.call-done = bf16[16,2048]{1,0:T(8,128)(2,1)} async-done(((bf16[16,2048]{1,0:T(8,128)(2,1)}), bf16[16,2048]{1,0:T(8,128)(2,1)}) %all-reduce.7.cloned.1.call-update) | async-done | bytes 65552 | tf_op jit(solution)/shard_map/psum | solution.py:33
  142.7 0.8 dynamic-slice_convert_fusion
  143.5 0.1 multiply_add_fusion.2
  143.7 0.0 copy-start.3
  143.7 2.6 %multiply_add_fusion.1 = (f32[1,4,4,128,128]{4,3,2,1,0:T(8,128)S(1)}, f32[1,4,4,128,128]{4,3,2,1,0:T(8,128)S(1)}) fusion(f32[2,4,4,128,128]{4,3,2,1,0:T(8,128)} %param.19, f32[4,4,128]{2,1,0:T(4,128)S(1)} %mul.268, f32[4,4,128]{2,1,0:T(4,128)S(1)} %mul.265, f32[4,4,128]{2,1,0:T(4,128)S(1)} %mul.261, f32[4,4,128]{2,1,0:T(4,128)S(1)} %mul.296, ...), kind=kLoop, calls=%fused_computation.28 | loop fusion | flops 1572864 | bytes 4243456 | tf_op jit(solution)/shard_map/add | solution.py:51
  146.3 0.0 copy-done.3
  146.3 0.7 fusion.2
  147.0 0.1 multiply_reduce_fusion.2
  147.1 0.1 multiply_bitcast_fusion
  147.2 0.1 fusion.44
  147.3 5.2 %all-gather.3 = bf16[4,4,512]{2,1,0:T(4,128)(2,1)S(1)} all-gather(bf16[1,4,512]{2,1,0:T(4,128)(2,1)S(1)} %fusion.44), channel_id=1, replica_groups=mesh['grp'=2,'tp'=4,'dp'=4] {'dp'}, dimensions={0}, use_global_device_ids=true | all-gather | bytes 20480 | tf_op jit(solution)/shard_map/all_gather | solution.py:66
  152.5 1.5 convolution_convert_fusion
  154.0 19.0 %all-reduce.1 = bf16[16,1024]{1,0:T(8,128)(2,1)S(1)} all-reduce(bf16[16,1024]{1,0:T(8,128)(2,1)S(1)} %convolution_convert_fusion), channel_id=3, replica_groups=mesh['grp'=2,'tp'=4,'dp'=4] {'tp'}, use_global_device_ids=true, to_apply=%region_9.0.clone | all-reduce | flops 16384 | bytes 65536
  173.0 0.6 add_convert_fusion
  173.6 1.5 pad_maximum_fusion
  (17 shorter events, 0.2 us)
Async XLA Ops:
  7.2 19.1 %copy-start.1 = (bf16[2,1024,512]{2,1,0:T(8,128)(2,1)S(1)}, bf16[2,1024,512]{2,1,0:T(8,128)(2,1)}, u32[]{:S(2)}) copy-start(bf16[2,1024,512]{2,1,0:T(8,128)(2,1)} %param.13) | copy-start | bytes 6291460
  7.2 54.3 %all-reduce.5.cloned.1.call-start = ((), (), s32[]{:S(2)}) async-start(), calls=%async_computation | async-start | bytes 131072 | tf_op jit(solution)/shard_map/psum | solution.py:33
  23.3 5.6 %copy-start.6 = (f32[2,128]{1,0:T(2,128)S(1)}, f32[2,128]{1,0:T(2,128)}, u32[]{:S(2)}) copy-start(f32[2,128]{1,0:T(2,128)} %param.17) | copy-start | bytes 3076
  23.3 5.6 %copy-start.5 = (f32[2,512]{1,0:T(2,128)S(1)}, f32[2,512]{1,0:T(2,128)}, u32[]{:S(2)}) copy-start(f32[2,512]{1,0:T(2,128)} %param.16) | copy-start | bytes 12292
  23.3 11.4 %copy-start.7 = (u32[32]{0:T(128)S(1)}, u32[32]{0:T(128)}, u32[]{:S(2)}) copy-start(u32[32]{0:T(128)} %constant.30) | copy-start | bytes 388
  26.5 63.8 %copy-start.4 = (bf16[4,1024]{1,0:T(4,128)(2,1)S(1)}, bf16[4,1024]{1,0:T(4,128)(2,1)}, u32[]{:S(2)}) copy-start(bf16[4,1024]{1,0:T(4,128)(2,1)} %param.10) | copy-start | bytes 24580
  26.5 77.1 %copy-start = (bf16[2,1024,512]{2,1,0:T(8,128)(2,1)S(1)}, bf16[2,1024,512]{2,1,0:T(8,128)(2,1)}, u32[]{:S(2)}) copy-start(bf16[2,1024,512]{2,1,0:T(8,128)(2,1)} %param.15) | copy-start | bytes 6291460
  28.8 113.9 %all-reduce.7.cloned.1.call-start = ((), (), s32[]{:S(2)}) async-start(), calls=%async_computation.1 | async-start | bytes 131072 | tf_op jit(solution)/shard_map/psum | solution.py:33
  103.5 2.1 %copy-start.2 = (bf16[2,1024,512]{2,1,0:T(8,128)(2,1)S(1)}, bf16[2,1024,512]{2,1,0:T(8,128)(2,1)}, u32[]{:S(2)}) copy-start(bf16[2,1024,512]{2,1,0:T(8,128)(2,1)} %param.13) | copy-start | bytes 6291460
  143.7 2.6 %copy-start.3 = (f32[2,4,4,128,128]{4,3,2,1,0:T(8,128)S(1)}, f32[2,4,4,128,128]{4,3,2,1,0:T(8,128)}, u32[]{:S(2)}) copy-start(f32[2,4,4,128,128]{4,3,2,1,0:T(8,128)} %param.19) | copy-start | bytes 6291460
Sparse Core Ops, SparseCore 0:
  28.9 32.5 all-reduce.4
  113.9 28.7 all-reduce.6
where the time goes:
time: 182 us
  blocking collectives  88.1 us (48%)
  waiting for transfers between devices  54.5 us (30%)
  between operations  14.9 us (8%)
  matrix products  14.1 us (8%)
  other arithmetic  8.64 us (5%)
    psum x2, waiting for transfers between devices, per_device(): lax.psum(payload[0].astype(jnp.bfloat16), 'dp').astype(jnp.float32)  54.4 us
    unnamed x2, blocking collectives  38 us
    all_gather x2, blocking collectives, per_device(): gathered = lax.all_gather(hidden, 'tp', axis=0, tiled=True)  28.2 us
    psum x2, blocking collectives, per_device(): square_total = lax.psum(squares, 'dp')  11.5 us
    all_gather x2, blocking collectives, per_device(): lax.all_gather(normed, 'dp', axis=0, tiled=True)  10.4 us
    dot_general x8, matrix products, per_device(): jnp.dot(scaled, weight[layer], preferred_element_type=jnp.float32)  8.47 us
  transfers between devices with their start and end apart: 2, of which 2 were waited for; matrix products, arithmetic and copies ran while one was open for 0% of the time, Pallas kernels for 0%

commit v1 on v0

--- a/solution.py
+++ b/solution.py
@@ -2,6 +2,7 @@
 import jax.numpy as jnp
 from jax import lax
 from jax.sharding import PartitionSpec as P
+from jax.lax import all_gather
 
 D = 4096
 HD = 128
@@ -27,7 +28,7 @@
             ],
             axis=1,
         )
-        square_total = lax.psum(squares, "dp")
+        square_total = jnp.sum(all_gather(squares, "dp"), 0)
         own_squares = lax.dynamic_slice_in_dim(square_total, offset, local_seqs, 0)
         payload = (joined,)
         summed = (lax.psum(payload[0].astype(jnp.bfloat16), "dp").astype(jnp.float32),)

time: 182 us -> 183 us (level)
    psum x2 -> x0, blocking collectives: 11.5 us -> none  [per_device(): square_total = lax.psum(squares, 'dp')]
    unnamed x2 -> x4, blocking collectives: 38 us -> 49.4 us
  transfers between devices with their start and end apart: 2 -> 2, of which waited for: 2 -> 2; matrix products, arithmetic and copies ran while one was open for 0% -> 1% of each run, Pallas kernels for 0% -> 0%
where the time goes in v1:
time: 183 us; the launch traced here: 182 us
  blocking collectives  88 us (48%)
  waiting for transfers between devices  52.9 us (29%)
  between operations  15.5 us (8%)
  matrix products  14.1 us (8%)
  other arithmetic  8.73 us (5%)
  local copies, waits for them, and re-layouts  2.88 us (2%)
    psum x2, waiting for transfers between devices, per_device(): lax.psum(payload[0].astype(jnp.bfloat16), 'dp').astype(jnp.float32)  52.9 us
    unnamed x4, blocking collectives  49.4 us
    all_gather x2, blocking collectives, per_device(): gathered = lax.all_gather(hidden, 'tp', axis=0, tiled=True)  28.2 us
    all_gather x2, blocking collectives, per_device(): lax.all_gather(normed, 'dp', axis=0, tiled=True)  10.4 us
    dot_general x8, matrix products, per_device(): jnp.dot(scaled, weight[layer], preferred_element_type=jnp.float32)  8.48 us
  transfers between devices with their start and end apart: 2, of which 2 were waited for; matrix products, arithmetic and copies ran while one was open for 1% of the time, Pallas kernels for 0%

profile of v1, /device:TPU:0, one launch (start us, length us, event | category | flops | bytes accessed | tf_op | source)
XLA Modules:
  0.0 182.2 jit_solution(7922369420570722631)
XLA Ops:
  7.2 0.0 copy-start.1
  7.2 0.0 all-reduce.7.cloned.1.call-start
  7.2 0.9 fusion.47
  8.1 15.1 %all-gather.2 = bf16[4,4,1024]{2,1,0:T(4,128)(2,1)S(1)} all-gather(bf16[1,4,1024]{2,1,0:T(4,128)(2,1)} %bitcast.93), channel_id=1, replica_groups=mesh['grp'=2,'tp'=4,'dp'=4] {'tp'}, dimensions={0}, use_global_device_ids=true | all-gather | bytes 40960 | tf_op jit(solution)/shard_map/all_gather | solution.py:20
  23.2 0.1 multiply_convert_fusion.1
  23.3 0.0 copy-start.5
  23.3 0.0 copy-start.8
  23.3 0.0 copy-start.7
  23.3 1.5 convolution_convert_fusion.6
  24.8 1.5 convolution_convert_fusion.7
  26.3 0.0 copy-done.1
  26.3 0.2 convolution_convert_fusion.8
  26.5 1.6 convolution_convert_fusion.9
  28.2 0.7 pad_maximum_fusion.1
  28.8 0.0 all-reduce.7.cloned.1.call-update
  28.8 0.0 all-reduce.9.cloned.1.call-start
  28.9 0.0 copy-done.6
  28.9 0.0 copy-done.5
  29.0 0.0 copy-done.8
  29.0 0.6 dynamic-slice
  30.2 0.2 dynamic-update-slice
  30.5 5.6 %all-reduce = f32[64]{0:T(128)S(1)} all-reduce(f32[64]{0:T(128)S(1)} %dynamic-update-slice), channel_id=2, replica_groups=mesh['grp'=2,'tp'=4,'dp'=4] {'dp'}, use_global_device_ids=true, to_apply=%add | all-reduce | flops 64 | bytes 512
  36.1 0.1 reshape.52
  36.2 0.1 add_rsqrt_fusion.3
  36.3 0.0 copy-done.7
  36.3 0.6 dynamic-slice.2
  37.5 24.0 %all-reduce.7.cloned.1.call-done = bf16[16,2048]{1,0:T(8,128)(2,1)} async-done(((bf16[16,2048]{1,0:T(8,128)(2,1)}), bf16[16,2048]{1,0:T(8,128)(2,1)}) %all-reduce.7.cloned.1.call-update) | async-done | bytes 65552 | tf_op jit(solution)/shard_map/psum | solution.py:34
  61.5 0.8 dynamic-slice_convert_fusion.1
  62.3 0.1 multiply_add_fusion.3
  62.4 1.9 %fusion.10 = f32[4,4,1,128]{3,2,1,0:T(1,128)S(1)} fusion(f32[4,4,128,1]{2,3,1,0:T(1,128)S(1)} %bitcast.101, f32[2,4,4,128,128]{4,3,2,1,0:T(8,128)} %param.19, f32[4,4,128]{2,1,0:T(4,128)S(1)} %mul.268, f32[4,4,128]{2,1,0:T(4,128)S(1)} %mul.265, f32[4,4,128]{2,1,0:T(4,128)S(1)} %mul.261), kind=kOutput, calls=%fused_computation.22 | convolution fusion | flops 1310720 | bytes 1089536 | tf_op jit(solution)/shard_map/bhkv,bhk->bhv/dot_general | solution.py:56
  64.4 0.1 multiply_reduce_fusion.3
  64.5 0.1 multiply_bitcast_fusion.1
  64.6 0.1 fusion.45
  64.7 5.2 %all-gather.3 = bf16[4,4,512]{2,1,0:T(4,128)(2,1)S(1)} all-gather(bf16[1,4,512]{2,1,0:T(4,128)(2,1)S(1)} %fusion.45), channel_id=1, replica_groups=mesh['grp'=2,'tp'=4,'dp'=4] {'dp'}, dimensions={0}, use_global_device_ids=true | all-gather | bytes 20480 | tf_op jit(solution)/shard_map/all_gather | solution.py:67
  69.9 1.5 convolution_convert_fusion.1
  71.4 19.0 %all-reduce.2 = bf16[16,1024]{1,0:T(8,128)(2,1)S(1)} all-reduce(bf16[16,1024]{1,0:T(8,128)(2,1)S(1)} %convolution_convert_fusion.1), channel_id=4, replica_groups=mesh['grp'=2,'tp'=4,'dp'=4] {'tp'}, use_global_device_ids=true, to_apply=%region_4.0.clone | all-reduce | flops 16384 | bytes 65536
  90.3 0.0 copy-done.4
  90.4 13.1 %all-gather.4 = bf16[4,4,1024]{2,1,0:T(4,128)(2,1)S(1)} all-gather(bf16[1,4,1024]{2,1,0:T(4,128)(2,1)S(1)} %fusion.46), channel_id=1, replica_groups=mesh['grp'=2,'tp'=4,'dp'=4] {'tp'}, dimensions={0}, use_global_device_ids=true | all-gather | bytes 40960 | tf_op jit(solution)/shard_map/all_gather | solution.py:20
  103.5 0.0 copy-start.2
  103.5 0.1 multiply_convert_fusion
  103.7 0.0 copy-done
  103.7 0.2 convolution_convert_fusion.2
  103.9 1.7 convolution_convert_fusion.3
  105.6 0.3 convolution_convert_fusion.4
  105.8 1.5 convolution_convert_fusion.5
  107.3 0.2 dynamic-update-slice.1
  107.5 5.8 %all-reduce.1 = f32[64]{0:T(128)S(1)} all-reduce(f32[64]{0:T(128)S(1)} %dynamic-update-slice.1), channel_id=3, replica_groups=mesh['grp'=2,'tp'=4,'dp'=4] {'dp'}, use_global_device_ids=true, to_apply=%add.1 | all-reduce | flops 64 | bytes 512
  113.4 0.1 reshape.53
  113.4 0.6 pad_maximum_fusion.2
  114.1 0.0 all-reduce.9.cloned.1.call-update
  114.1 0.1 add_rsqrt_fusion.2
  114.2 28.8 %all-reduce.9.cloned.1.call-done = bf16[16,2048]{1,0:T(8,128)(2,1)} async-done(((bf16[16,2048]{1,0:T(8,128)(2,1)}), bf16[16,2048]{1,0:T(8,128)(2,1)}) %all-reduce.9.cloned.1.call-update) | async-done | bytes 65552 | tf_op jit(solution)/shard_map/psum | solution.py:34
  143.0 0.8 dynamic-slice_convert_fusion
  143.8 0.1 multiply_add_fusion.2
  144.0 2.6 %multiply_add_fusion.1 = (f32[1,4,4,128,128]{4,3,2,1,0:T(8,128)S(1)}, f32[1,4,4,128,128]{4,3,2,1,0:T(8,128)S(1)}) fusion(f32[2,4,4,128,128]{4,3,2,1,0:T(8,128)} %param.19, f32[4,4,128]{2,1,0:T(4,128)S(1)} %mul.268, f32[4,4,128]{2,1,0:T(4,128)S(1)} %mul.265, f32[4,4,128]{2,1,0:T(4,128)S(1)} %mul.261, f32[4,4,128]{2,1,0:T(4,128)S(1)} %mul.296, ...), kind=kLoop, calls=%fused_computation.28 | loop fusion | flops 1572864 | bytes 4243456 | tf_op jit(solution)/shard_map/add | solution.py:52
  146.6 0.7 fusion.2
  147.3 0.1 multiply_reduce_fusion.2
  147.4 0.1 multiply_bitcast_fusion
  147.5 0.1 fusion.44
  147.6 5.2 %all-gather.5 = bf16[4,4,512]{2,1,0:T(4,128)(2,1)S(1)} all-gather(bf16[1,4,512]{2,1,0:T(4,128)(2,1)S(1)} %fusion.44), channel_id=1, replica_groups=mesh['grp'=2,'tp'=4,'dp'=4] {'dp'}, dimensions={0}, use_global_device_ids=true | all-gather | bytes 20480 | tf_op jit(solution)/shard_map/all_gather | solution.py:67
  152.8 1.5 convolution_convert_fusion
  154.3 19.0 %all-reduce.3 = bf16[16,1024]{1,0:T(8,128)(2,1)S(1)} all-reduce(bf16[16,1024]{1,0:T(8,128)(2,1)S(1)} %convolution_convert_fusion), channel_id=5, replica_groups=mesh['grp'=2,'tp'=4,'dp'=4] {'tp'}, use_global_device_ids=true, to_apply=%region_9.0.clone | all-reduce | flops 16384 | bytes 65536
  173.3 0.6 add_convert_fusion
  173.9 1.5 pad_maximum_fusion
  (27 shorter events, 0.3 us)
Async XLA Ops:
  7.2 19.1 %copy-start.1 = (bf16[2,1024,512]{2,1,0:T(8,128)(2,1)S(1)}, bf16[2,1024,512]{2,1,0:T(8,128)(2,1)}, u32[]{:S(2)}) copy-start(bf16[2,1024,512]{2,1,0:T(8,128)(2,1)} %param.13) | copy-start | bytes 6291460
  7.2 54.4 %all-reduce.7.cloned.1.call-start = ((), (), s32[]{:S(2)}) async-start(), calls=%async_computation | async-start | bytes 131072 | tf_op jit(solution)/shard_map/psum | solution.py:34
  23.3 5.6 %copy-start.6 = (f32[2,128]{1,0:T(2,128)S(1)}, f32[2,128]{1,0:T(2,128)}, u32[]{:S(2)}) copy-start(f32[2,128]{1,0:T(2,128)} %param.17) | copy-start | bytes 3076
  23.3 5.6 %copy-start.5 = (f32[2,512]{1,0:T(2,128)S(1)}, f32[2,512]{1,0:T(2,128)}, u32[]{:S(2)}) copy-start(f32[2,512]{1,0:T(2,128)} %param.16) | copy-start | bytes 12292
  23.3 5.7 %copy-start.8 = (u32[32]{0:T(128)S(1)}, u32[32]{0:T(128)}, u32[]{:S(2)}) copy-start(u32[32]{0:T(128)} %constant.30) | copy-start | bytes 388
  23.3 13.0 %copy-start.7 = (u32[32]{0:T(128)S(1)}, u32[32]{0:T(128)}, u32[]{:S(2)}) copy-start(u32[32]{0:T(128)} %constant.42) | copy-start | bytes 388
  26.5 63.8 %copy-start.4 = (bf16[4,1024]{1,0:T(4,128)(2,1)S(1)}, bf16[4,1024]{1,0:T(4,128)(2,1)}, u32[]{:S(2)}) copy-start(bf16[4,1024]{1,0:T(4,128)(2,1)} %param.10) | copy-start | bytes 24580
  26.5 77.1 %copy-start = (bf16[2,1024,512]{2,1,0:T(8,128)(2,1)S(1)}, bf16[2,1024,512]{2,1,0:T(8,128)(2,1)}, u32[]{:S(2)}) copy-start(bf16[2,1024,512]{2,1,0:T(8,128)(2,1)} %param.15) | copy-start | bytes 6291460
  28.8 114.2 %all-reduce.9.cloned.1.call-start = ((), (), s32[]{:S(2)}) async-start(), calls=%async_computation.1 | async-start | bytes 131072 | tf_op jit(solution)/shard_map/psum | solution.py:34
  103.5 2.1 %copy-start.2 = (bf16[2,1024,512]{2,1,0:T(8,128)(2,1)S(1)}, bf16[2,1024,512]{2,1,0:T(8,128)(2,1)}, u32[]{:S(2)}) copy-start(bf16[2,1024,512]{2,1,0:T(8,128)(2,1)} %param.13) | copy-start | bytes 6291460
  144.0 2.6 %copy-start.3 = (f32[2,4,4,128,128]{4,3,2,1,0:T(8,128)S(1)}, f32[2,4,4,128,128]{4,3,2,1,0:T(8,128)}, u32[]{:S(2)}) copy-start(f32[2,4,4,128,128]{4,3,2,1,0:T(8,128)} %param.19) | copy-start | bytes 6291460
Sparse Core Ops, SparseCore 0:
  29.0 32.5 all-reduce.6
  114.2 28.7 all-reduce.8
